TPU v7x, 32 devices: a whole 2x2x4 slice. The times are simulated.
32 devices in a mesh: sp: 16 (over z, y, x), tp: 2 (over core).
Axes of the slice: x: 2, y: 2, z: 4, core: 2. Of those that a mesh axis runs over, the one named last changes fastest.
Arguments:
- tokens: bfloat16 [4096, 2048], P(('sp', 'tp')), may hold values from -6 to 6
- norm_gain: float32 [2048], replicated, may hold values from 0.1 to 1.9
- w_query: bfloat16 [2048, 1024], P('sp', 'tp'), may hold values from -0.125 to 0.125
- w_forget: bfloat16 [2048, 1024], P('sp', 'tp'), may hold values from -0.125 to 0.125
- w_value: bfloat16 [2048, 1024], P('sp', 'tp'), may hold values from -0.125 to 0.125
- w_outgate: bfloat16 [2048, 1024], P('sp', 'tp'), may hold values from -0.125 to 0.125
- leak: float32 [1024], P('tp'), may hold values from 4.8828126e-05 to 0.00024414062
- decay_shift: float32 [4096, 1024], P('sp', 'tp'), may hold values from -1 to 0
- head_gain: float32 [128], replicated, may hold values from 0.1 to 1.9
- w_glu_value: bfloat16 [2048, 2048], P('sp', 'tp'), may hold values from -0.125 to 0.125
- w_glu_gate: bfloat16 [2048, 2048], P('sp', 'tp'), may hold values from -0.125 to 0.125
- conv_kernel: float32 [31, 2048], P(None, 'tp'), may hold values from -20 to 20
- ln_gain: float32 [2048], P('tp'), may hold values from 0.1 to 1.9
- ln_bias: float32 [2048], P('tp'), may hold values from -3 to 3
- w_out_rec: bfloat16 [1024, 2048], P('tp', 'sp'), may hold values from -0.125 to 0.125
- w_out_conv: bfloat16 [2048, 2048], P('tp', 'sp'), may hold values from -0.09375 to 0.09375
Outputs:
- mixed: bfloat16 [4096, 2048], P(('sp', 'tp'))
All inputs are finite; a program needn't handle non-finite values.
Results may differ from a plain program's by a relative error of at most 0.019.
Values may be sent and summed in bfloat16 or wider, within the bound.
A program may use at most 64 MiB of HBM per device.

v0:
```python
import jax
import jax.numpy as jnp
from jax import lax
from jax.sharding import PartitionSpec as P

HEAD_K = 128
HEAD_V = 128
KERNEL = 31
BLOCK = 64


exact_precision = lax.Precision.HIGHEST


def prefix(value, axis, combine, identity):
    peers, position = (lax.axis_size(axis), lax.axis_index(axis))
    everything = jax.tree.map(
        lambda part, kind: lax.all_gather(part.astype(kind), axis),
        value,
        (jnp.bfloat16, jnp.bfloat16),
    )
    start = jax.tree.map(
        lambda part, zero: jnp.broadcast_to(jnp.asarray(zero, part.dtype), part.shape),
        value,
        identity,
    )

    def turn(k, before):
        reached = k < position
        new = combine(
            before, jax.tree.map(lambda part, own: part[k].astype(own.dtype), everything, value)
        )
        return jax.tree.map(lambda a, b: jnp.where(reached, a, b), new, before)

    return lax.fori_loop(0, peers, turn, start)


def from_behind(value, axis, steps):
    count = lax.axis_size(axis)
    initial, last = (max(0, -steps), min(count, count - steps))
    return lax.ppermute(value, axis, [(source, source + steps) for source in range(initial, last)])


def normalize(row_block, norm_gain):
    values_in = row_block.astype(jnp.float32)
    row_scale = lax.rsqrt(jnp.mean(values_in * values_in, axis=1, keepdims=True) + 1e-06)
    return (values_in * row_scale * norm_gain).astype(jnp.bfloat16)


def combine_states(earlier, later):
    return (earlier[0] + later[0], jnp.exp(later[0])[..., None] * earlier[1] + later[1])


def local_recurrence(queries, in_gate, payload_matrix_lines, log_decay):
    row_count, head_count, key_width = queries.shape
    value_width = payload_matrix_lines.shape[2]
    block_count = row_count // BLOCK

    def split_blocks(tensor):
        return tensor.reshape(block_count, BLOCK, head_count, tensor.shape[-1])

    q_blocks = split_blocks(queries)
    k_blocks = split_blocks(in_gate)
    v_blocks = split_blocks(payload_matrix_lines)
    cumulative_sum = jnp.cumsum(split_blocks(log_decay), axis=1)
    causal = jnp.tril(jnp.ones((BLOCK, BLOCK), jnp.float32))
    scores = jnp.einsum(
        "nthk,nshk->nhts",
        q_blocks * jnp.exp(cumulative_sum),
        k_blocks * jnp.exp(-cumulative_sum),
        precision=exact_precision,
    )
    within = jnp.einsum("nhts,nshv->nthv", scores * causal, v_blocks, precision=exact_precision)
    block_finish = cumulative_sum[:, -1]
    contrib = jnp.einsum(
        "nshk,nshv->nhkv",
        k_blocks * jnp.exp(block_finish[:, None] - cumulative_sum),
        v_blocks,
        precision=exact_precision,
    )

    def advance(carried_in, inputs):
        state_list, before = carried_in
        query_block, column_block, e_block, added_terms = inputs
        carried_state = jnp.einsum(
            "aub,ubd->aud",
            query_block * jnp.exp(column_block),
            state_list,
            precision=exact_precision,
        )
        device_query = query_block * jnp.exp(column_block + before[None])
        state_list = jnp.exp(e_block)[..., None] * state_list + added_terms
        return ((state_list, before + e_block), (carried_state, device_query))

    initial = (
        jnp.zeros((head_count, key_width, value_width), jnp.float32),
        jnp.zeros((head_count, key_width), jnp.float32),
    )
    (state_list, totals), (carried_state, device_query) = lax.scan(
        advance, initial, (q_blocks, cumulative_sum, block_finish, contrib)
    )
    recurrence_step = (within + carried_state).reshape(row_count, head_count, value_width)
    return (
        recurrence_step,
        device_query.reshape(row_count, head_count, key_width),
        state_list,
        totals,
    )


def on_device(
    tokens,
    norm_gain,
    w_query,
    w_forget,
    w_value,
    w_outgate,
    leak,
    decay_shift,
    head_gain,
    w_glu_value,
    w_glu_gate,
    conv_kernel,
    ln_gain,
    ln_bias,
    w_out_rec,
    w_out_conv,
):
    widths = [
        w_query.shape[1],
        w_forget.shape[1],
        w_value.shape[1],
        w_outgate.shape[1],
        w_glu_value.shape[1],
        w_glu_gate.shape[1],
    ]
    gathered = (
        lax.all_gather(w_query, "sp", axis=0, tiled=True),
        lax.all_gather(w_forget, "sp", axis=0, tiled=True),
        lax.all_gather(w_value, "sp", axis=0, tiled=True),
        lax.all_gather(w_outgate, "sp", axis=0, tiled=True),
        lax.all_gather(w_glu_value, "sp", axis=0, tiled=True),
        lax.all_gather(w_glu_gate, "sp", axis=0, tiled=True),
        lax.all_gather(w_out_rec, "sp", axis=1, tiled=True),
        lax.all_gather(w_out_conv, "sp", axis=1, tiled=True),
    )
    full_in = gathered[:6]
    out_rec = gathered[6]
    out_conv = gathered[7]
    normed = normalize(lax.all_gather(tokens, "tp", axis=0, tiled=True), norm_gain)
    joined = jnp.concatenate(
        [
            jnp.dot(normed, weight, preferred_element_type=jnp.float32).astype(jnp.bfloat16)
            for weight in full_in
        ],
        axis=1,
    )
    projections = []
    column = 0
    for width_now in widths:
        projections.append(joined[:, column : column + width_now])
        column = column + width_now
    query_pre, forget_pre, value_pre, gate_pre, glu_value_pre, glu_gate_pre = projections
    row_count = query_pre.shape[0]
    head_count = query_pre.shape[1] // HEAD_K
    queries = jax.nn.silu(query_pre.astype(jnp.float32))
    in_gate = leak * jax.nn.sigmoid(-forget_pre.astype(jnp.float32))
    log_decay = jnp.log1p(-in_gate) + decay_shift
    recurrence_step, device_query, state_list, totals = local_recurrence(
        queries.reshape(row_count, head_count, HEAD_K),
        in_gate.reshape(row_count, head_count, HEAD_K),
        value_pre.astype(jnp.float32).reshape(row_count, head_count, HEAD_V),
        log_decay.reshape(row_count, head_count, HEAD_K),
    )
    _, incoming_state = prefix(
        (totals, state_list),
        "sp",
        combine_states,
        (jnp.zeros_like(totals), jnp.zeros_like(state_list)),
    )
    recurrence_step = recurrence_step + jnp.einsum(
        "aub,ubd->aud", device_query, incoming_state, precision=exact_precision
    )
    scaling = lax.rsqrt(jnp.mean(recurrence_step * recurrence_step, axis=2, keepdims=True) + 1e-06)
    gate_act = jax.nn.silu(gate_pre.astype(jnp.float32)).reshape(row_count, head_count, HEAD_V)
    head_out = (
        (recurrence_step * scaling * head_gain * gate_act)
        .reshape(row_count, head_count * HEAD_V)
        .astype(jnp.bfloat16)
    )
    glu = (
        glu_value_pre.astype(jnp.float32) * jax.nn.sigmoid(glu_gate_pre.astype(jnp.float32))
    ).astype(jnp.bfloat16)
    left_rim = from_behind(glu[row_count - (KERNEL - 1) :], "sp", 1)
    extended = jnp.concatenate([left_rim, glu], axis=0).astype(jnp.float32)

    def add_tap(tap_index, accum):
        taps = lax.dynamic_slice_in_dim(conv_kernel, tap_index, 1, 0)
        return accum + taps * lax.dynamic_slice_in_dim(extended, tap_index, row_count, 0)

    conv_sum = lax.fori_loop(0, KERNEL, add_tap, jnp.zeros((row_count, glu.shape[1]), jnp.float32))
    channel_count = conv_sum.shape[1] * lax.axis_size("tp")
    sum_rows, square_rows = lax.psum(
        (
            jnp.sum(conv_sum, axis=1, keepdims=True),
            jnp.sum(conv_sum * conv_sum, axis=1, keepdims=True),
        ),
        "tp",
    )
    row_mean = sum_rows / channel_count
    centered = conv_sum - row_mean
    row_var = square_rows / channel_count - row_mean * row_mean
    conv_out = jax.nn.silu(centered * lax.rsqrt(row_var + 1e-05) * ln_gain + ln_bias).astype(
        jnp.bfloat16
    )
    return lax.psum_scatter(
        (
            jnp.dot(head_out, out_rec, preferred_element_type=jnp.float32)
            + jnp.dot(conv_out, out_conv, preferred_element_type=jnp.float32)
        ).astype(jnp.bfloat16),
        "tp",
        scatter_dimension=0,
        tiled=True,
    )


def solution(mesh):
    placed = (
        P(("sp", "tp"), None),
        P(),
        P("sp", "tp"),
        P("sp", "tp"),
        P("sp", "tp"),
        P("sp", "tp"),
        P("tp"),
        P("sp", "tp"),
        P(),
        P("sp", "tp"),
        P("sp", "tp"),
        P(None, "tp"),
        P("tp"),
        P("tp"),
        P("tp", "sp"),
        P("tp", "sp"),
    )
    return jax.shard_map(
        on_device, mesh=mesh, in_specs=placed, out_specs=P(("sp", "tp"), None), check_vma=False
    )
```

profile of v0, /device:TPU:0, one launch (start us, length us, event | category | flops | bytes accessed | tf_op | source)
XLA Modules:
  0.0 657.1 jit_solution(7365507671859252702)
XLA Ops:
  10.0 10.7 %all-gather.14.cloned.1.call-done = bf16[256,2048]{1,0:T(8,128)(2,1)} async-done(((bf16[128,2048]{1,0:T(8,128)(2,1)}), bf16[256,2048]{1,0:T(8,128)(2,1)}) %all-gather.14.cloned.1.call-update) | async-done | bytes 1048592 | tf_op jit(solution)/shard_map/all_gather | solution.py:150
  20.7 1.5 fusion.12
  22.2 62.8 %all-gather.20.cloned.1.call-done = bf16[2048,512]{1,0:T(8,128)(2,1)} async-done(((bf16[128,512]{1,0:T(8,128)(2,1)}), bf16[2048,512]{1,0:T(8,128)(2,1)}) %all-gather.20.cloned.1.call-update) | async-done | bytes 2097168 | tf_op jit(solution)/shard_map/all_gather | solution.py:139
  85.0 2.9 log-plus-one_add_fusion
  88.5 58.5 %all-gather.18.cloned.1.call-done = bf16[2048,512]{1,0:T(8,128)(2,1)} async-done(((bf16[128,512]{1,0:T(8,128)(2,1)}), bf16[2048,512]{1,0:T(8,128)(2,1)}) %all-gather.18.cloned.1.call-update) | async-done | bytes 2097168 | tf_op jit(solution)/shard_map/all_gather | solution.py:138
  147.0 2.8 divide_multiply_fusion.1
  150.0 58.9 %all-gather.16.cloned.1.call-done = bf16[2048,512]{1,0:T(8,128)(2,1)} async-done(((bf16[128,512]{1,0:T(8,128)(2,1)}), bf16[2048,512]{1,0:T(8,128)(2,1)}) %all-gather.16.cloned.1.call-update) | async-done | bytes 2097168 | tf_op jit(solution)/shard_map/all_gather | solution.py:140
  208.8 2.7 convolution_convert_fusion.5
  211.6 1.2 exponential_multiply_fusion.1
  212.8 1.0 fusion.33
  213.8 7.8 %while.45 = (s32[]{:T(128)}, f32[4,128,128]{2,1,0:T(8,128)S(1)}, f32[4,128]{1,0:T(4,128)S(1)}, f32[4,64,4,128]{3,1,2,0:T(8,128)}, f32[4,64,4,128]{3,1,0,2:T(8,12...) while((s32[]{:T(128)}, f32[4,128,128]{2,1,0:T(8,128)S(1)}, ...), condition=%wide.region_3.4_spmd.clone, body=%wide.region_2.3_spmd.clone.sunk | while | flops 50693120 | bytes 2374789 | solution.py:99
  214.6 1.0 fusion.73
  216.5 1.0 fusion.73
  218.5 1.0 fusion.73
  220.5 1.0 fusion.73
  225.3 38.8 %all-gather.2 = bf16[16,4,128]{2,1,0:T(4,128)(2,1)S(1)} all-gather(bf16[1,4,128]{2,1,0:T(4,128)(2,1)S(1)} %convert_bitcast_fusion), channel_id=2, replica_groups=mesh['sp'=16,'tp'=2] {'sp'}, dimensions={0}, use_global_device_ids=true | all-gather | bytes 17408 | tf_op jit(solution)/shard_map/all_gather | solution.py:18
  264.1 2.0 convolution_multiply_fusion
  266.8 3.9 all-gather.22.cloned.1.call-done
  270.7 2.8 divide_multiply_fusion
  273.7 58.9 %all-gather.32.cloned.1.call-done = bf16[64,128,128]{2,1,0:T(8,128)(2,1)} async-done(((bf16[4,128,128]{2,1,0:T(8,128)(2,1)}), bf16[64,128,128]{2,1,0:T(8,128)(2,1)}) %all-gather.32.cloned.1.call-update) | async-done | bytes 2097168 | tf_op jit(solution)/shard_map/all_gather | solution.py:18
  332.6 18.4 %while.46 = (s32[]{:T(128)}, f32[4,128,128]{2,1,0:T(8,128)S(1)}, s32[]{:T(128)}, bf16[16,4,128]{2,1,0:T(4,128)(2,1)S(1)}, bf16[16,4,128,128]{3,2,1,0:T(8,128)(2,1)}, /*index=5*/s32[]{:T(128)}, s32[]{:T(128)}) while((s32[]{:T(128)}, f32[4,128,128]{2,1,0:T(8,128)S(1)}, s32[]{:T(128)}, bf16[16,4,128]{2,1,0:T(4,128)(2,1)S(1)}, ...), condition=%wide.region_5.6_spmd.clone, body=%wide.region_4.5_spmd.clone.sunk | while | flops 328196 | bytes 660585 | solution.py:35
  332.6 1.1 fusion.74
  333.7 1.1 fusion.74
  334.9 1.1 fusion.74
  336.0 1.1 fusion.74
  337.2 1.1 fusion.74
  338.3 1.1 fusion.74
  339.5 1.1 fusion.74
  340.6 1.1 fusion.74
  341.8 1.1 fusion.74
  342.9 1.1 fusion.74
  344.1 1.1 fusion.74
  345.2 1.1 fusion.74
  346.4 1.1 fusion.74
  347.5 1.1 fusion.74
  348.7 1.1 fusion.74
  349.8 1.1 fusion.74
  350.9 1.7 multiply_reduce_fusion.1
  352.7 57.1 %all-gather.26.cloned.1.call-done = bf16[2048,1024]{1,0:T(8,128)(2,1)} async-done(((bf16[128,1024]{1,0:T(8,128)(2,1)}), bf16[2048,1024]{1,0:T(8,128)(2,1)}) %all-gather.26.cloned.1.call-update) | async-done | bytes 4194320 | tf_op jit(solution)/shard_map/all_gather | solution.py:142
  409.8 4.8 fusion.22
  414.6 72.2 %all-gather.28.cloned.1.call-done = bf16[2048,1024]{1,0:T(8,128)(2,1)} async-done(((bf16[128,1024]{1,0:T(8,128)(2,1)}), bf16[2048,1024]{1,0:T(8,128)(2,1)}) %all-gather.28.cloned.1.call-update) | async-done | bytes 4194320 | tf_op jit(solution)/shard_map/all_gather | solution.py:143
  486.8 4.2 fusion.21
  491.0 3.5 collective-permute-start
  494.6 1.6 collective-permute-done
  496.4 40.1 %while.47 = (s32[]{:T(128)}, f32[256,1024]{1,0:T(8,128)S(1)}, f32[31,1024]{1,0:T(8,128)}, f32[286,1024]{1,0:T(8,128)S(1)}, s32[]{:T(128)}, /*index=5*/s32[]{:T(128)}) while((s32[]{:T(128)}, f32[256,1024]{1,0:T(8,128)S(1)}, f32[31,1024]{1,0:T(8,128)}, f32[286,1024]{1,0:T(8,128)S(1)}, s32[]{:T(128)}, /*index=5*/s32[]{:T(128)}) %tuple.92), condition=%wide.region_8.9_spmd.clone, body=%wide.region_7.8_spmd.clone.sunk | while | flops 786435 | bytes 3158103 | solution.py:201
  496.4 0.8 constant_dynamic-slice_fusion.6
  497.7 0.8 constant_dynamic-slice_fusion.6
  499.0 0.8 constant_dynamic-slice_fusion.6
  500.3 0.8 constant_dynamic-slice_fusion.6
  501.6 0.8 constant_dynamic-slice_fusion.6
  502.9 0.8 constant_dynamic-slice_fusion.6
  504.2 0.8 constant_dynamic-slice_fusion.6
  510.6 0.8 constant_dynamic-slice_fusion.6
  518.4 0.8 constant_dynamic-slice_fusion.6
  519.7 0.8 constant_dynamic-slice_fusion.6
  521.0 0.8 constant_dynamic-slice_fusion.6
  526.2 0.8 constant_dynamic-slice_fusion.6
  528.7 0.8 constant_dynamic-slice_fusion.6
  536.7 2.5 all-reduce
  539.2 37.6 %all-gather.30.cloned.1.call-done = bf16[1024,2048]{1,0:T(8,128)(2,1)} async-done(((bf16[1024,128]{1,0:T(8,128)(2,1)}), bf16[1024,2048]{1,0:T(8,128)(2,1)}) %all-gather.30.cloned.1.call-update) | async-done | bytes 4194320 | tf_op jit(solution)/shard_map/all_gather | solution.py:145
  576.8 3.7 fusion.32
  580.5 60.0 %all-gather.24.cloned.1.call-done = bf16[512,2048]{1,0:T(8,128)(2,1)} async-done(((bf16[512,128]{1,0:T(8,128)(2,1)}), bf16[512,2048]{1,0:T(8,128)(2,1)}) %all-gather.24.cloned.1.call-update) | async-done | bytes 2097168 | tf_op jit(solution)/shard_map/all_gather | solution.py:144
  640.5 3.3 fusion.11
  643.9 6.7 %reduce-scatter.2.cloned.1.call-done = bf16[128,2048]{1,0:T(8,128)(2,1)} async-done(((bf16[256,2048]{1,0:T(8,128)(2,1)}), bf16[128,2048]{1,0:T(8,128)(2,1)}) %reduce-scatter.2.cloned.1.call-update) | async-done | bytes 524304 | tf_op jit(solution)/shard_map/reduce_scatter | solution.py:216
  (143 shorter events, 42.2 us)
Async XLA Ops:
  6.5 78.5 %copy-start.3 = (f32[2048]{0:T(1024)S(1)}, f32[2048]{0:T(1024)}, u32[]{:S(2)}) copy-start(f32[2048]{0:T(1024)} %param.23) | copy-start | bytes 24580
  6.5 78.5 %copy-start.6 = (f32[512]{0:T(512)S(1)}, f32[512]{0:T(512)}, u32[]{:S(2)}) copy-start(f32[512]{0:T(512)} %param.28) | copy-start | bytes 6148
  6.5 78.5 %copy-start.2 = (f32[256,512]{1,0:T(8,128)S(1)}, f32[256,512]{1,0:T(8,128)}, u32[]{:S(2)}) copy-start(f32[256,512]{1,0:T(8,128)} %param.29) | copy-start | bytes 1572868
  6.5 14.1 %all-gather.14.cloned.1.call-start = ((), (), s32[]{:S(2)}) async-start(), calls=%async_computation.1 | async-start | bytes 1572864 | tf_op jit(solution)/shard_map/all_gather | solution.py:150
  7.3 77.8 %all-gather.20.cloned.1.call-start = ((), (), s32[]{:S(2)}) async-start(), calls=%async_computation.4 | async-start | bytes 2228224 | tf_op jit(solution)/shard_map/all_gather | solution.py:139
  8.0 139.0 %all-gather.18.cloned.1.call-start = ((), (), s32[]{:S(2)}) async-start(), calls=%async_computation.3 | async-start | bytes 2228224 | tf_op jit(solution)/shard_map/all_gather | solution.py:138
  8.7 200.1 %all-gather.16.cloned.1.call-start = ((), (), s32[]{:S(2)}) async-start(), calls=%async_computation.2 | async-start | bytes 2228224 | tf_op jit(solution)/shard_map/all_gather | solution.py:140
  9.3 261.4 %all-gather.22.cloned.1.call-start = ((), (), s32[]{:S(2)}) async-start(), calls=%async_computation.5 | async-start | bytes 2228224 | tf_op jit(solution)/shard_map/all_gather | solution.py:141
  9.9 322.7 %all-gather.32.cloned.1.call-start = ((), (), s32[]{:S(2)}) async-start(), calls=%async_computation.11 | async-start | bytes 2228224 | tf_op jit(solution)/shard_map/all_gather | solution.py:18
  221.7 44.5 %copy-start = (f32[4,64,4,128]{3,1,2,0:T(8,128)S(1)}, f32[4,64,4,128]{3,1,2,0:T(8,128)}, u32[]{:S(2)}) copy-start(f32[4,64,4,128]{3,1,2,0:T(8,128)} %get-tuple-element.228) | copy-start | bytes 1572868
  222.4 187.4 %all-gather.26.cloned.1.call-start = ((), (), s32[]{:S(2)}) async-start(), calls=%async_computation.7 | async-start | bytes 4456448 | tf_op jit(solution)/shard_map/all_gather | solution.py:142
  223.1 263.6 %all-gather.28.cloned.1.call-start = ((), (), s32[]{:S(2)}) async-start(), calls=%async_computation.8 | async-start | bytes 4456448 | tf_op jit(solution)/shard_map/all_gather | solution.py:143
  223.9 352.9 %all-gather.30.cloned.1.call-start = ((), (), s32[]{:S(2)}) async-start(), calls=%async_computation.9 | async-start | bytes 4456448 | tf_op jit(solution)/shard_map/all_gather | solution.py:145
  224.6 415.9 %all-gather.24.cloned.1.call-start = ((), (), s32[]{:S(2)}) async-start(), calls=%async_computation.6 | async-start | bytes 2228224 | tf_op jit(solution)/shard_map/all_gather | solution.py:144
  225.2 425.4 %reduce-scatter.2.cloned.1.call-start = ((), (), s32[]{:S(2)}) async-start(), calls=%async_computation.10 | async-start | bytes 1572864 | tf_op jit(solution)/shard_map/reduce_scatter | solution.py:216
  414.6 79.9 %copy-start.1 = (f32[128]{0:T(128)S(1)}, f32[128]{0:T(128)}, u32[]{:S(2)}) copy-start(f32[128]{0:T(128)} %param.30) | copy-start | bytes 1540
  491.0 5.2 collective-permute-start
  496.4 80.4 %copy-start.4 = (f32[1024]{0:T(1024)S(1)}, f32[1024]{0:T(1024)}, u32[]{:S(2)}) copy-start(f32[1024]{0:T(1024)} %param.35) | copy-start | bytes 12292
  496.4 80.4 %copy-start.5 = (f32[1024]{0:T(1024)S(1)}, f32[1024]{0:T(1024)}, u32[]{:S(2)}) copy-start(f32[1024]{0:T(1024)} %param.34) | copy-start | bytes 12292
Sparse Core Ops, SparseCore 0:
  8.9 11.7 all-gather.13
  23.4 61.5 all-gather.19
  87.8 59.1 all-gather.17
  149.6 59.1 all-gather.15
  211.5 59.2 all-gather.21
  273.4 59.1 all-gather.31
  335.3 74.3 all-gather.25
  412.5 74.1 all-gather.27
  489.5 87.3 all-gather.29
  579.4 61.1 all-gather.23
  644.0 6.5 reduce-scatter.1
where the time goes:
time: 660 us; the launch traced here: 657 us
  waiting for transfers between devices  495 us (75%)
  blocking collectives  41.3 us (6%)
  other arithmetic  41 us (6%)
  matrix products  36.4 us (6%)
  local copies, waits for them, and re-layouts  25 us (4%)
  between operations  13.5 us (2%)
    all_gather x1, waiting for transfers between devices, on_device(): lax.all_gather(w_glu_gate, 'sp', axis=0, tiled=True)  72.2 us
    all_gather x1, waiting for transfers between devices, on_device(): lax.all_gather(w_forget, 'sp', axis=0, tiled=True)  62.8 us
    all_gather x1, waiting for transfers between devices, on_device(): lax.all_gather(w_out_rec, 'sp', axis=1, tiled=True)  60 us
    all_gather x1, waiting for transfers between devices, on_device(): lax.all_gather(w_value, 'sp', axis=0, tiled=True)  58.9 us
    all_gather x1, waiting for transfers between devices, prefix(): lax.all_gather(part.astype(kind), axis)  58.9 us
    all_gather x1, waiting for transfers between devices, on_device(): lax.all_gather(w_query, 'sp', axis=0, tiled=True)  58.5 us
    all_gather x1, waiting for transfers between devices, on_device(): lax.all_gather(w_glu_value, 'sp', axis=0, tiled=True)  57.1 us
    all_gather x1, blocking collectives, prefix(): lax.all_gather(part.astype(kind), axis)  38.8 us
  transfers between devices with their start and end apart: 12, of which 12 were waited for; matrix products, arithmetic and copies ran while one was open for 15% of the time, Pallas kernels for 0%

commit v1 on v0

v1 whole, which is shorter than its diff:
```python
import jax
import jax.numpy as jnp
from jax import lax
from jax.experimental import pallas as pl
from jax.experimental.pallas import tpu as pltpu
from jax.sharding import PartitionSpec as P

HEAD_K = 128
HEAD_V = 128
KERNEL = 31
HALO = 32
BLOCK = 64
MESH = pl.DeviceIdType.MESH


exact_precision = lax.Precision.HIGHEST


def exchange(x, kind, group, scatter, collective_id):
    lines = lax.axis_size("sp") // group
    cores = lax.axis_size("tp")
    count = {"line": lines, "plane": group, "core": cores, "all": group * cores}[kind]
    shape = x.shape if scatter else (count,) + x.shape
    if count == 1:
        return x.reshape(shape)

    def body(x_ref, o_ref, send_sem, recv_sem, local_sem):
        sp, core = lax.axis_index("sp"), lax.axis_index("tp")
        line, spot = sp // group, sp % group

        def where(m):
            return {
                "line": lambda: (m * group + spot, core),
                "plane": lambda: (line * group + m, core),
                "core": lambda: (sp, m),
                "all": lambda: (line * group + m // cores, m % cores),
            }[kind]()

        me = {"line": line, "plane": spot, "core": core, "all": spot * cores + core}[kind]
        others = [lax.rem(me + d, count) for d in range(1, count)]
        barrier = pltpu.get_barrier_semaphore()
        for other in others:
            pl.semaphore_signal(barrier, inc=1, device_id=where(other), device_id_type=MESH)
        pl.semaphore_wait(barrier, count - 1)
        copies = []
        for d, other in enumerate(others):
            copy = pltpu.make_async_remote_copy(
                src_ref=x_ref.at[other] if scatter else x_ref,
                dst_ref=o_ref.at[me],
                send_sem=send_sem.at[d],
                recv_sem=recv_sem.at[d],
                device_id=where(other),
                device_id_type=MESH,
            )
            copy.start()
            copies.append(copy)
        own = pltpu.make_async_copy(x_ref.at[me] if scatter else x_ref, o_ref.at[me], local_sem)
        own.start()
        own.wait()
        for copy in copies:
            copy.wait()

    return pl.pallas_call(
        body,
        out_shape=jax.ShapeDtypeStruct(shape, x.dtype),
        in_specs=[pl.BlockSpec(memory_space=pltpu.VMEM)],
        out_specs=pl.BlockSpec(memory_space=pltpu.VMEM),
        scratch_shapes=[
            pltpu.SemaphoreType.DMA((count,)),
            pltpu.SemaphoreType.DMA((count,)),
            pltpu.SemaphoreType.DMA,
        ],
        compiler_params=pltpu.CompilerParams(collective_id=collective_id, has_side_effects=True),
    )(x)


def spread(pieces, rows, group, collective_id):
    slots = lax.axis_size("sp")
    lines = slots // group
    cores = lax.axis_size("tp")
    peers = group * cores

    def body(
        w_ref, t_ref, w_all, t_all,
        plane_send, up_send, down_send, w_recv, t_send, t_recv, local_sem,
    ):
        sp, core = lax.axis_index("sp"), lax.axis_index("tp")
        line, spot = sp // group, sp % group
        seat = spot * cores + core
        has_up, has_down = line + 1 < lines, line > 0
        barrier = pltpu.get_barrier_semaphore()

        def greet(device):
            pl.semaphore_signal(barrier, inc=1, device_id=device, device_id_type=MESH)

        def place(m):
            return (line * group + m // cores, m % cores)

        others = [lax.rem(seat + d, peers) for d in range(1, peers)]
        for other in others:
            greet(place(other))

        @pl.when(has_up)
        def _():
            greet((sp + group, core))

        @pl.when(has_down)
        def _():
            greet((sp - group, core))

        met = peers - 1 + has_up.astype(jnp.int32) + has_down.astype(jnp.int32)
        pl.semaphore_wait(barrier, met)

        def remote(src, dst, send_sem, recv_sem, device):
            return pltpu.make_async_remote_copy(
                src_ref=src, dst_ref=dst, send_sem=send_sem, recv_sem=recv_sem,
                device_id=device, device_id_type=MESH,
            )

        own = pltpu.make_async_copy(w_ref.at[spot], w_all.at[sp], local_sem.at[0])
        own.start()
        started = []
        for d in range(1, group):
            to = lax.rem(spot + d, group)
            copy = remote(
                w_ref.at[to], w_all.at[sp], plane_send.at[d], w_recv.at[sp],
                (line * group + to, core),
            )
            copy.start()
            started.append(copy)
        own_rows = pltpu.make_async_copy(t_ref, t_all.at[seat], local_sem.at[1])
        own_rows.start()
        row_copies = []
        for d, other in enumerate(others):
            copy = remote(t_ref, t_all.at[seat], t_send.at[d], t_recv.at[d], place(other))
            copy.start()
            row_copies.append(copy)

        def up(slot):
            return remote(
                w_all.at[slot], w_all.at[slot], up_send.at[slot], w_recv.at[slot],
                (sp + group, core),
            )

        def down(slot):
            return remote(
                w_all.at[slot], w_all.at[slot], down_send.at[slot], w_recv.at[slot],
                (sp - group, core),
            )

        def arrive(slot, device):
            remote(
                w_all.at[slot], w_all.at[slot], up_send.at[slot], w_recv.at[slot], device
            ).wait_recv()

        own.wait()
        for d in range(lines):
            for k in range(group):
                if d == 0:
                    slot = line * group + lax.rem(spot + k, group)
                    if k > 0:
                        arrive(slot, (slot, core))

                    @pl.when(has_up)
                    def _():
                        up(slot).start()

                    @pl.when(has_down)
                    def _():
                        down(slot).start()
                else:
                    low = (line - d) * group + lax.rem(spot + k, group)
                    high = (line + d) * group + lax.rem(spot + k, group)

                    @pl.when(line >= d)
                    def _():
                        arrive(low, (sp - group, core))

                        @pl.when(has_up)
                        def _():
                            up(low).start()

                    @pl.when(line + d < lines)
                    def _():
                        arrive(high, (sp + group, core))

                        @pl.when(has_down)
                        def _():
                            down(high).start()

        own_rows.wait()
        for copy in row_copies:
            copy.wait()
        for copy in started:
            copy.wait_send()
        for d in range(lines):
            for k in range(group):
                low = (line - d) * group + k
                high = (line + d) * group + k

                @pl.when((line >= d) & has_up)
                def _():
                    up(low).wait_send()

                @pl.when((line + d < lines) & has_down)
                def _():
                    down(high).wait_send()

    return pl.pallas_call(
        body,
        out_shape=(
            jax.ShapeDtypeStruct((slots,) + pieces.shape[1:], pieces.dtype),
            jax.ShapeDtypeStruct((peers,) + rows.shape, rows.dtype),
        ),
        in_specs=[pl.BlockSpec(memory_space=pltpu.VMEM)] * 2,
        out_specs=[pl.BlockSpec(memory_space=pltpu.VMEM)] * 2,
        scratch_shapes=[
            pltpu.SemaphoreType.DMA((group,)),
            pltpu.SemaphoreType.DMA((slots,)),
            pltpu.SemaphoreType.DMA((slots,)),
            pltpu.SemaphoreType.DMA((slots,)),
            pltpu.SemaphoreType.DMA((peers,)),
            pltpu.SemaphoreType.DMA((peers,)),
            pltpu.SemaphoreType.DMA((2,)),
        ],
        compiler_params=pltpu.CompilerParams(
            collective_id=collective_id, has_side_effects=True, vmem_limit_bytes=48 * 2**20
        ),
    )(pieces, rows)


def depthwise(extended, taps):
    rows = extended.shape[0] - HALO
    channels = extended.shape[1]
    step = 64
    wide = 128

    def body(x_ref, k_ref, o_ref):
        for column in range(0, channels, wide):
            here = slice(column, column + wide)

            @pl.loop(0, rows // step)
            def _(turn):
                base = pl.multiple_of(turn * step, step)
                chunk = x_ref[pl.ds(base, step + HALO), here]
                total = jnp.zeros((step, wide), jnp.float32)
                for phase in range(8):
                    turned = chunk if phase == 0 else pltpu.roll(chunk, step + HALO - phase, 0)
                    for start in range(0, HALO + 8, 8):
                        j = start + phase - (HALO - (KERNEL - 1))
                        if 0 <= j < KERNEL:
                            total = total + k_ref[j : j + 1, here] * turned[start : start + step]
                o_ref[pl.ds(base, step), here] = total

    return pl.pallas_call(
        body,
        out_shape=jax.ShapeDtypeStruct((rows, channels), jnp.float32),
        in_specs=[pl.BlockSpec(memory_space=pltpu.VMEM)] * 2,
        out_specs=pl.BlockSpec(memory_space=pltpu.VMEM),
        cost_estimate=pl.CostEstimate(
            flops=2 * KERNEL * rows * channels, bytes_accessed=8 * rows * channels, transcendentals=0
        ),
    )(extended, taps)


def normalize(row_block, norm_gain):
    values_in = row_block.astype(jnp.float32)
    row_scale = lax.rsqrt(jnp.mean(values_in * values_in, axis=1, keepdims=True) + 1e-06)
    return (values_in * row_scale * norm_gain).astype(jnp.bfloat16)


def recurrence(queries, in_gate, value, log_decay, group):
    rows, width = queries.shape
    blocks = rows // BLOCK
    q, k, v, a = (
        t.reshape(blocks, BLOCK, t.shape[1]) for t in (queries, in_gate, value, log_decay)
    )
    causal = jnp.tril(jnp.ones((BLOCK, BLOCK), jnp.float32))
    running = jnp.einsum("ts,nsk->ntk", causal, a, precision=exact_precision)
    finish = running[:, -1]
    q_in = (q * jnp.exp(running)).astype(jnp.bfloat16)
    k_out = (k * jnp.exp(-running)).astype(jnp.bfloat16)
    k_end = (k * jnp.exp(finish[:, None] - running)).astype(jnp.bfloat16)
    scores = jnp.einsum("ntk,nsk->nts", q_in, k_out, preferred_element_type=jnp.float32)
    within = jnp.einsum(
        "nts,nsv->ntv", (scores * causal).astype(jnp.bfloat16), v, preferred_element_type=jnp.float32
    )
    added = jnp.einsum("nsk,nsv->nkv", k_end, v, preferred_element_type=jnp.float32)
    after = jnp.cumsum(finish[::-1], axis=0)[::-1]
    total = after[0]
    tail = jnp.exp(after - finish)
    local_state = jnp.sum(tail[..., None] * added, axis=0)
    sent = jnp.concatenate([local_state, jnp.broadcast_to(total[None], (8, width))], axis=0)
    gathered = exchange(sent, "line", group, False, 1)
    line = lax.axis_index("sp") // group
    state = jnp.zeros_like(local_state)
    for m in range(gathered.shape[0]):
        grown = jnp.exp(gathered[m, width])[:, None] * state + gathered[m, :width]
        state = jnp.where(m < line, grown, state)
    before = []
    factor = jnp.exp(finish)
    for n in range(blocks):
        before.append(state.astype(jnp.bfloat16))
        state = factor[n][:, None] * state + added[n]
    carried = jnp.einsum(
        "ntk,nkv->ntv", q_in, jnp.stack(before), preferred_element_type=jnp.float32
    )
    return (within + carried).reshape(rows, value.shape[1])


def on_device(
    tokens,
    norm_gain,
    w_query,
    w_forget,
    w_value,
    w_outgate,
    leak,
    decay_shift,
    head_gain,
    w_glu_value,
    w_glu_gate,
    conv_kernel,
    ln_gain,
    ln_bias,
    w_out_rec,
    w_out_conv,
):
    bf16 = jnp.bfloat16
    slots, cores = lax.axis_size("sp"), lax.axis_size("tp")
    group = w_query.shape[1] // HEAD_K
    spot = lax.axis_index("sp") % group
    depth = w_query.shape[0]
    width = w_out_rec.shape[1]
    channels = w_glu_value.shape[1] // group
    inner = HEAD_V + channels
    total_width = 4 * HEAD_K + 2 * channels

    def by_spot(weight):
        return weight.reshape(depth, group, -1)

    pieces = jnp.concatenate(
        [by_spot(w) for w in (w_query, w_forget, w_value, w_outgate, w_glu_value, w_glu_gate)],
        axis=2,
    ).transpose(1, 0, 2)
    out_pieces = jnp.concatenate(
        [w_out_rec.reshape(group, HEAD_V, width), w_out_conv.reshape(group, channels, width)], axis=1
    )
    folds = total_width // width
    out_pieces = (
        out_pieces.reshape(group, folds, inner // folds, width)
        .transpose(0, 2, 1, 3)
        .reshape(group, inner // folds, total_width)
    )
    everything, normed = spread(
        jnp.concatenate([pieces, out_pieces], axis=1), normalize(tokens, norm_gain), group, 0
    )
    shift_all = exchange(
        decay_shift.reshape(decay_shift.shape[0], group, HEAD_K).transpose(1, 0, 2),
        "plane", group, True, 2,
    )
    rows = normed.shape[0] * normed.shape[1]
    normed = normed.reshape(rows, normed.shape[2])
    shift = shift_all.reshape(rows, HEAD_K)
    full_in = everything[:, :depth].reshape(slots * depth, total_width)
    full_out = (
        everything[:, depth:]
        .reshape(slots, inner // folds, folds, width)
        .transpose(2, 1, 0, 3)
        .reshape(inner, slots * width)
    )
    joined = jnp.dot(normed, full_in, preferred_element_type=jnp.float32).astype(bf16)
    query_pre, forget_pre, value_pre, gate_pre = (
        joined[:, n * HEAD_K : (n + 1) * HEAD_K] for n in range(4)
    )
    glu_value_pre = joined[:, 4 * HEAD_K : 4 * HEAD_K + channels]
    glu_gate_pre = joined[:, 4 * HEAD_K + channels :]

    glu = (
        glu_value_pre.astype(jnp.float32) * jax.nn.sigmoid(glu_gate_pre.astype(jnp.float32))
    ).astype(bf16)
    rim = lax.ppermute(
        glu[rows - HALO :], "sp", [(s, s + group) for s in range(slots - group)]
    )
    extended = jnp.concatenate([rim, glu], axis=0).astype(jnp.float32)
    mine = lambda t: lax.dynamic_slice_in_dim(t, spot * channels, channels, t.ndim - 1)
    conv_sum = depthwise(extended, mine(conv_kernel))
    sums = jnp.stack([jnp.sum(conv_sum, axis=1), jnp.sum(conv_sum * conv_sum, axis=1)])
    sums = jnp.sum(exchange(sums, "all", group, False, 3), axis=0)
    channel_count = channels * group * cores
    row_mean = sums[0][:, None] / channel_count
    row_var = sums[1][:, None] / channel_count - row_mean * row_mean
    conv_out = jax.nn.silu(
        (conv_sum - row_mean) * lax.rsqrt(row_var + 1e-05) * mine(ln_gain) + mine(ln_bias)
    ).astype(bf16)

    queries = jax.nn.silu(query_pre.astype(jnp.float32))
    own_leak = lax.dynamic_slice_in_dim(leak, spot * HEAD_K, HEAD_K, 0)
    in_gate = own_leak * jax.nn.sigmoid(-forget_pre.astype(jnp.float32))
    log_decay = jnp.log1p(-in_gate) + shift
    recur = recurrence(queries, in_gate, value_pre, log_decay, group)
    scaling = lax.rsqrt(jnp.mean(recur * recur, axis=1, keepdims=True) + 1e-06)
    head_out = (recur * scaling * head_gain * jax.nn.silu(gate_pre.astype(jnp.float32))).astype(bf16)

    partial = jnp.dot(
        jnp.concatenate([head_out, conv_out], axis=1), full_out, preferred_element_type=jnp.float32
    ).astype(bf16)
    own_rows = tokens.shape[0]
    by_core = partial.reshape(group, cores, own_rows, -1).transpose(1, 0, 2, 3)
    by_plane = exchange(by_core, "core", group, True, 4)
    by_plane = jnp.sum(by_plane.astype(jnp.float32), axis=0).astype(bf16)
    back = exchange(by_plane, "plane", group, True, 5)
    return jnp.sum(back.astype(jnp.float32), axis=0).astype(bf16)


def solution(mesh):
    placed = (
        P(("sp", "tp"), None),
        P(),
        P("sp", "tp"),
        P("sp", "tp"),
        P("sp", "tp"),
        P("sp", "tp"),
        P("tp"),
        P("sp", "tp"),
        P(),
        P("sp", "tp"),
        P("sp", "tp"),
        P(None, "tp"),
        P("tp"),
        P("tp"),
        P("tp", "sp"),
        P("tp", "sp"),
    )
    return jax.shard_map(
        on_device, mesh=mesh, in_specs=placed, out_specs=P(("sp", "tp"), None), check_vma=False
    )
```

time: 660 us -> 246 us (0.37)
  waiting for transfers between devices: 495 us -> 0.01 us
  Pallas kernels: 0 us -> 179 us
  blocking collectives: 41.3 us -> 0 us
  matrix products: 36.4 us -> 9.97 us
  between operations: 13.5 us -> 0.65 us
  local copies, waits for them, and re-layouts: 25 us -> 17.8 us
    all_gather x10 -> x0, waiting for transfers between devices: 481 us -> none  [the longest x1 72.2 us: on_device(): lax.all_gather(w_glu_gate, 'sp', axis=0, tiled=True)]
    pallas_call x0 -> x7, Pallas kernels: none -> 179 us  [the longest x1 111 us: spread(): pl.pallas_call(body, out_shape=(jax.ShapeDtypeStruct((slots,) + pieces.sh...]
    all_gather x1 -> x0, blocking collectives: 38.8 us -> none  [prefix(): lax.all_gather(part.astype(kind), axis)]
    dot_general x16 -> x6, matrix products: 36.4 us -> 9.97 us  [the longest x1 4.71 us: on_device(): jnp.dot(normed, full_in, preferred_element_type=jnp.float32).astype(bf16)]
    dynamic_slice x35 -> x4, local copies, waits for them, and re-layouts: 23.9 us -> 2.91 us  [the longest x3 2.15 us: on_device(): lax.dynamic_slice_in_dim(t, spot * channels, channels, t.ndim - 1)]
    select_n x17 -> x1, other arithmetic: 17.7 us -> 0.01 us  [recurrence(): causal = jnp.tril(jnp.ones((BLOCK, BLOCK), jnp.float32))]
    add x39 -> x0, other arithmetic: 16.4 us -> none  [the longest x31 15.7 us: add_tap(): accum + taps * lax.dynamic_slice_in_dim(extended, tap_index, row_count, 0)]
    unnamed x5 -> x15, other arithmetic: 0.01 us -> 14.5 us
  transfers between devices with their start and end apart: 12 -> 1, of which waited for: 12 -> 0; matrix products, arithmetic and copies ran while one was open for 15% -> 13% of each run, Pallas kernels for 0% -> 8%
where the time goes in v1:
time: 246 us; the launch traced here: 244 us
  Pallas kernels  179 us (73%)
  other arithmetic  35.4 us (14%)
  local copies, waits for them, and re-layouts  17.8 us (7%)
  matrix products  9.97 us (4%)
    pallas_call x1, Pallas kernels, spread(): pl.pallas_call(body, out_shape=(jax.ShapeDtypeStruct((slots,) + pieces.sh...  111 us
    pallas_call x5, Pallas kernels, exchange(): pl.pallas_call(body, out_shape=jax.ShapeDtypeStruct(shape, x.dtype), in_s...  62.1 us
    unnamed x15, other arithmetic  14.5 us
    pallas_call x1, Pallas kernels, depthwise(): pl.pallas_call(body, out_shape=jax.ShapeDtypeStruct((rows, channels), jnp...  5.78 us
    reduce_sum x1, other arithmetic, on_device(): by_plane = jnp.sum(by_plane.astype(jnp.float32), axis=0).astype(bf16)  5.07 us
  transfers between devices with their start and end apart: 1, of which 0 were waited for; matrix products, arithmetic and copies ran while one was open for 13% of the time, Pallas kernels for 8%

profile of v1, /device:TPU:0, one launch (start us, length us, event | category | flops | bytes accessed | tf_op | source)
XLA Modules:
  0.0 244.5 jit_solution(3182544345083318625)
XLA Ops:
  0.0 1.1 pad_maximum_fusion.1
  1.2 1.0 copy.17
  3.3 0.2 copy.21
  3.5 0.1 copy.27
  3.6 0.2 copy.22
  3.8 0.1 copy.28
  4.0 0.2 fusion.3
  4.5 0.5 copy-done.9
  5.0 0.2 fusion.5.t_ref
  5.2 111.2 %shard_map.154 = (bf16[16,176,1024]{2,1,0:T(8,128)(2,1)}, bf16[8,128,2048]{2,1,0:T(8,128)(2,1)S(1)}) custom-call(bf16[4,176,1024]{2,1,0:T(8,128)(2,1)S(1)} %pad_maximum_fusion.w_ref, bf16[128,2048]{1,0:T(8,128)(2,1)S(1)} %fusion.5.t_ref), custom_call_target="tpu_custom_call" | custom-call | tf_op jit(solution)/shard_map/pallas_call | solution.py:209
  116.4 2.6 %slice.184 = bf16[16,128,1024]{2,1,0:T(8,128)(2,1)S(1)} slice(bf16[16,176,1024]{2,1,0:T(8,128)(2,1)} %get-tuple-element.8), slice={[0:16], [0:128], [0:1024]} | slice | bytes 8388608 | tf_op jit(solution)/shard_map/slice | solution.py:365
  119.0 4.7 %convolution_convert_fusion.1 = bf16[1024,1024]{1,0:T(8,128)(2,1)S(1)} fusion(bf16[1024,2048]{1,0:T(8,128)(2,1)S(1)} %bitcast.108, bf16[2048,1024]{1,0:T(8,128)(2,1)S(1)} %bitcast.115), kind=kOutput, calls=%fused_computation.2 | convolution fusion | flops 4296015872 | bytes 10485760 | tf_op jit(solution)/shard_map/dot_general | solution.py:372
  123.7 1.3 copy-done.1
  125.0 0.3 multiply_convert_fusion.1
  125.4 1.6 collective-permute-start
  127.0 0.2 copy.30
  127.2 1.0 copy.31
  128.2 9.5 %shard_map.155 = f32[4,256,128]{2,1,0:T(8,128)} custom-call(f32[4,256,128]{2,1,0:T(8,128)} %bitcast.120), custom_call_target="tpu_custom_call" | custom-call | tf_op jit(solution)/shard_map/pallas_call | solution.py:63
  137.7 0.8 dynamic_slice.12
  138.5 1.6 divide_multiply_fusion
  140.1 0.7 multiply_convert_fusion.4
  140.9 1.0 slice.252
  141.9 1.5 multiply_reduce_fusion.1
  143.4 0.6 pad_maximum_fusion.2.x_ref
  144.0 8.8 %shard_map.156 = f32[4,136,128]{2,1,0:T(8,128)} custom-call(f32[136,128]{1,0:T(8,128)} %pad_maximum_fusion.2.x_ref), custom_call_target="tpu_custom_call" | custom-call | tf_op jit(solution)/shard_map/pallas_call | solution.py:63
  152.9 0.7 exponential_bitcast_fusion.2
  153.6 1.1 constant_dynamic-update-slice_fusion.21
  154.7 0.9 constant_dynamic-update-slice_fusion.20
  155.6 1.0 constant_dynamic-update-slice_fusion.19
  156.6 0.9 constant_dynamic-update-slice_fusion.18
  157.5 1.0 constant_dynamic-update-slice_fusion.17
  158.5 0.9 constant_dynamic-update-slice_fusion.16
  159.5 1.0 constant_dynamic-update-slice_fusion.15
  160.5 0.9 constant_dynamic-update-slice_fusion.14
  161.4 1.0 constant_dynamic-update-slice_fusion.13
  162.4 0.9 constant_dynamic-update-slice_fusion.12
  163.3 1.0 constant_dynamic-update-slice_fusion.11
  164.3 0.9 constant_dynamic-update-slice_fusion.10
  165.3 1.0 constant_dynamic-update-slice_fusion.9
  166.2 0.9 constant_dynamic-update-slice_fusion.8
  167.2 1.0 constant_dynamic-update-slice_fusion.7
  168.2 0.9 constant_dynamic-update-slice_fusion.6
  169.1 0.3 fusion.30
  169.4 0.5 multiply_reduce_fusion.2
  170.0 1.2 fusion.17
  171.2 0.6 constant_dynamic-slice_fusion.k_ref
  171.9 1.6 slice.249
  173.4 0.4 copy.35
  173.9 1.0 copy.32
  174.9 0.8 dynamic_slice.15
  175.7 0.8 dynamic_slice.14
  176.4 1.1 maximum_convert_fusion.x_ref
  177.5 5.8 %shard_map.157 = f32[1024,256]{1,0:T(8,128)} custom-call(f32[1056,256]{1,0:T(8,128)} %maximum_convert_fusion.x_ref, f32[31,256]{1,0:T(8,128)} %constant_dynamic-slice_fusion.k_ref), custom_call_target="tpu_custom_call" | custom-call | flops 16252928 | bytes 2097152 | tf_op jit(solution)/shard_map/pallas_call | solution.py:255
  183.3 1.6 fusion.28
  184.9 0.6 pad_maximum_fusion.3.x_ref
  185.5 6.5 %shard_map.158 = f32[8,2,1024]{2,1,0:T(2,128)} custom-call(f32[2,1024]{1,0:T(2,128)} %pad_maximum_fusion.3.x_ref), custom_call_target="tpu_custom_call" | custom-call | tf_op jit(solution)/shard_map/pallas_call | solution.py:63
  191.9 0.9 reduce_sum.83
  192.9 1.6 multiply_convert_fusion
  194.5 2.3 convolution_convert_fusion
  196.9 2.3 copy.43
  199.1 8.3 %shard_map.159 = bf16[2,4,128,2048]{3,2,1,0:T(8,128)(2,1)} custom-call(bf16[2,4,128,2048]{3,2,1,0:T(8,128)(2,1)} %bitcast.109), custom_call_target="tpu_custom_call" | custom-call | tf_op jit(solution)/shard_map/pallas_call | solution.py:63
  207.5 5.1 %reduce_sum.84.x_ref = bf16[4,128,2048]{2,1,0:T(8,128)(2,1)} reduce(bf16[2,4,128,2048]{3,2,1,0:T(8,128)(2,1)} %shard_map.159, bf16[]{:T(256)} %constant.77.clone.1), dimensions={0}, to_apply=%region_7.8 | reduce | flops 1048576 | bytes 6291458 | tf_op jit(solution)/shard_map/reduce_sum | solution.py:411
  212.5 29.0 %shard_map.160 = bf16[4,128,2048]{2,1,0:T(8,128)(2,1)} custom-call(bf16[4,128,2048]{2,1,0:T(8,128)(2,1)} %reduce_sum.84.x_ref), custom_call_target="tpu_custom_call" | custom-call | tf_op jit(solution)/shard_map/pallas_call | solution.py:63
  241.5 2.9 %reduce_sum.85 = bf16[128,2048]{1,0:T(8,128)(2,1)} reduce(bf16[4,128,2048]{2,1,0:T(8,128)(2,1)} %shard_map.160, bf16[]{:T(256)} %constant.77.clone.1), dimensions={0}, to_apply=%region_8.9 | reduce | flops 786432 | bytes 2621442 | tf_op jit(solution)/shard_map/reduce_sum | solution.py:413
  (51 shorter events, 1.6 us)
Async XLA Ops:
  0.0 171.2 %copy-start = (f32[31,1024]{1,0:T(8,128)S(1)}, f32[31,1024]{1,0:T(8,128)}, u32[]{:S(2)}) copy-start(f32[31,1024]{1,0:T(8,128)} %param.27) | copy-start | bytes 380932
  0.0 2.4 %copy-start.6 = (bf16[128,512]{1,0:T(8,128)(2,1)S(1)}, bf16[128,512]{1,0:T(8,128)(2,1)}, u32[]{:S(2)}) copy-start(bf16[128,512]{1,0:T(8,128)(2,1)} %param.19) | copy-start | bytes 393220
  0.0 2.7 %copy-start.7 = (bf16[128,512]{1,0:T(8,128)(2,1)S(1)}, bf16[128,512]{1,0:T(8,128)(2,1)}, u32[]{:S(2)}) copy-start(bf16[128,512]{1,0:T(8,128)(2,1)} %param.20) | copy-start | bytes 393220
  0.0 3.0 %copy-start.8 = (bf16[128,512]{1,0:T(8,128)(2,1)S(1)}, bf16[128,512]{1,0:T(8,128)(2,1)}, u32[]{:S(2)}) copy-start(bf16[128,512]{1,0:T(8,128)(2,1)} %param.21) | copy-start | bytes 393220
  0.0 3.3 %copy-start.4 = (bf16[128,1024]{1,0:T(8,128)(2,1)S(1)}, bf16[128,1024]{1,0:T(8,128)(2,1)}, u32[]{:S(2)}) copy-start(bf16[128,1024]{1,0:T(8,128)(2,1)} %param.25) | copy-start | bytes 786436
  1.1 2.5 %copy-start.5 = (bf16[128,1024]{1,0:T(8,128)(2,1)S(1)}, bf16[128,1024]{1,0:T(8,128)(2,1)}, u32[]{:S(2)}) copy-start(bf16[128,1024]{1,0:T(8,128)(2,1)} %param.26) | copy-start | bytes 786436
  2.3 1.7 copy-start.2
  4.3 0.7 copy-start.9
  119.0 8.0 %copy-start.3 = (f32[256,512]{1,0:T(8,128)S(1)}, f32[256,512]{1,0:T(8,128)}, u32[]{:S(2)}) copy-start(f32[256,512]{1,0:T(8,128)} %param.23) | copy-start | bytes 1572868
  123.7 1.3 copy-start.1
  125.4 51.1 %collective-permute-start = (bf16[32,256]{1,0:T(8,128)(2,1)S(1)}, bf16[32,256]{1,0:T(8,128)(2,1)S(1)}, u32[]{:S(2)}, u32[]{:S(2)}) collective-permute-start(bf16[32,256]{1,0:T(8,128)(2,1)S(1)} %slice.288), channel_id=1, source_target_pairs={{0,8},{2,10},{4,12},{6,14},{8,16},{10,18},{12,20},{14,22},{16,24},... | collective-permute-start | bytes 49160 | tf_op jit(solution)/shard_map/ppermute | solution.py:382
  168.2 1.8 copy-start.10

commit v2 on v1

--- a/solution.py
+++ b/solution.py
@@ -269,6 +269,25 @@
     return (values_in * row_scale * norm_gain).astype(jnp.bfloat16)
 
 
+def carry_through(q_in, added, factor, state):
+    blocks = q_in.shape[0]
+
+    def body(q_ref, add_ref, factor_ref, state_ref, o_ref):
+        now = state_ref[...]
+        for n in range(blocks):
+            o_ref[n] = jnp.dot(
+                q_ref[n], now.astype(jnp.bfloat16), preferred_element_type=jnp.float32
+            )
+            now = factor_ref[:, n : n + 1] * now + add_ref[n]
+
+    return pl.pallas_call(
+        body,
+        out_shape=jax.ShapeDtypeStruct(q_in.shape[:2] + state.shape[1:], jnp.float32),
+        in_specs=[pl.BlockSpec(memory_space=pltpu.VMEM)] * 4,
+        out_specs=pl.BlockSpec(memory_space=pltpu.VMEM),
+    )(q_in, added, factor, state)
+
+
 def recurrence(queries, in_gate, value, log_decay, group):
     rows, width = queries.shape
     blocks = rows // BLOCK
@@ -297,14 +316,7 @@
     for m in range(gathered.shape[0]):
         grown = jnp.exp(gathered[m, width])[:, None] * state + gathered[m, :width]
         state = jnp.where(m < line, grown, state)
-    before = []
-    factor = jnp.exp(finish)
-    for n in range(blocks):
-        before.append(state.astype(jnp.bfloat16))
-        state = factor[n][:, None] * state + added[n]
-    carried = jnp.einsum(
-        "ntk,nkv->ntv", q_in, jnp.stack(before), preferred_element_type=jnp.float32
-    )
+    carried = carry_through(q_in, added, jnp.exp(finish).T, state)
     return (within + carried).reshape(rows, value.shape[1])
 
 

time: 246 us -> 262 us (1.065)
  local copies, waits for them, and re-layouts: 17.8 us -> 34.7 us
  other arithmetic: 35.4 us -> 32.2 us
  Pallas kernels: 179 us -> 182 us
    unnamed x15 -> x0, other arithmetic: 14.5 us -> none
    convert_element_type x0 -> x1, other arithmetic: none -> 7.05 us  [recurrence(): k_out = (k * jnp.exp(-running)).astype(jnp.bfloat16)]
    convert_element_type x0 -> x3, local copies, waits for them, and re-layouts: none -> 5.67 us  [the longest x1 2.67 us: recurrence(): q_in = (q * jnp.exp(running)).astype(jnp.bfloat16)]
    reshape x0 -> x2, local copies, waits for them, and re-layouts: none -> 5.35 us  [recurrence(): t.reshape(blocks, BLOCK, t.shape[1])]
    dot_general x0 -> x1, local copies, waits for them, and re-layouts: none -> 2.7 us  [recurrence(): running = jnp.einsum('ts,nsk->ntk', causal, a, precision=exact_precision)]
    unnamed x35 -> x37, local copies, waits for them, and re-layouts: 4.35 us -> 5.33 us
  transfers between devices with their start and end apart: 1 -> 1, of which waited for: 0 -> 0; matrix products, arithmetic and copies ran while one was open for 13% -> 17% of each run, Pallas kernels for 8% -> 8%
where the time goes in v2:
time: 262 us; the launch traced here: 261 us
  Pallas kernels  182 us (69%)
  local copies, waits for them, and re-layouts  34.7 us (13%)
  other arithmetic  32.2 us (12%)
  matrix products  10.6 us (4%)
    pallas_call x1, Pallas kernels, spread(): pl.pallas_call(body, out_shape=(jax.ShapeDtypeStruct((slots,) + pieces.sh...  111 us
    pallas_call x5, Pallas kernels, exchange(): pl.pallas_call(body, out_shape=jax.ShapeDtypeStruct(shape, x.dtype), in_s...  62.1 us
    convert_element_type x1, other arithmetic, recurrence(): k_out = (k * jnp.exp(-running)).astype(jnp.bfloat16)  7.05 us
    pallas_call x1, Pallas kernels, depthwise(): pl.pallas_call(body, out_shape=jax.ShapeDtypeStruct((rows, channels), jnp...  5.78 us
    reshape x2, local copies, waits for them, and re-layouts, recurrence(): t.reshape(blocks, BLOCK, t.shape[1])  5.35 us
    unnamed x37, local copies, waits for them, and re-layouts  5.33 us
  transfers between devices with their start and end apart: 1, of which 0 were waited for; matrix products, arithmetic and copies ran while one was open for 17% of the time, Pallas kernels for 8%

profile of v2, /device:TPU:0, one launch (start us, length us, event | category | flops | bytes accessed | tf_op | source)
XLA Modules:
  0.0 261.1 jit_solution(13381309604146970034)
XLA Ops:
  0.0 1.1 pad_maximum_fusion.1
  1.3 1.0 copy.52
  2.3 0.1 copy.58
  2.5 1.0 copy.53
  3.5 0.1 copy.59
  3.7 0.1 copy.54
  3.8 0.1 copy.60
  3.9 0.1 copy.55
  4.1 0.1 copy.61
  4.2 0.2 copy.56
  4.4 0.1 copy.62
  4.5 0.2 copy.57
  4.7 0.1 copy.63
  4.9 0.2 fusion.3
  5.4 0.2 fusion.5.t_ref
  5.6 111.2 %shard_map.154 = (bf16[16,176,1024]{2,1,0:T(8,128)(2,1)}, bf16[8,128,2048]{2,1,0:T(8,128)(2,1)S(1)}) custom-call(bf16[4,176,1024]{2,1,0:T(8,128)(2,1)S(1)} %pad_maximum_fusion.w_ref, bf16[128,2048]{1,0:T(8,128)(2,1)S(1)} %fusion.5.t_ref), custom_call_target="tpu_custom_call" | custom-call | tf_op jit(solution)/shard_map/pallas_call | solution.py:209
  116.8 2.6 %slice.64 = bf16[16,128,1024]{2,1,0:T(8,128)(2,1)S(1)} slice(bf16[16,176,1024]{2,1,0:T(8,128)(2,1)} %get-tuple-element.8), slice={[0:16], [0:128], [0:1024]} | slice | bytes 8388608 | tf_op jit(solution)/shard_map/slice | solution.py:377
  119.5 4.7 %convolution_convert_fusion.1 = bf16[1024,1024]{1,0:T(8,128)(2,1)S(1)} fusion(bf16[1024,2048]{1,0:T(8,128)(2,1)S(1)} %bitcast.107, bf16[2048,1024]{1,0:T(8,128)(2,1)S(1)} %bitcast.114), kind=kOutput, calls=%fused_computation.5 | convolution fusion | flops 4296015872 | bytes 10485760 | tf_op jit(solution)/shard_map/dot_general | solution.py:384
  124.2 0.3 multiply_convert_fusion.4
  124.5 0.9 slice.93
  125.4 1.4 collective-permute-start
  126.9 2.0 copy.65
  128.9 2.1 copy.66
  130.9 9.5 %shard_map.155 = f32[4,256,128]{2,1,0:T(8,128)} custom-call(f32[4,256,128]{2,1,0:T(8,128)} %bitcast.119), custom_call_target="tpu_custom_call" | custom-call | tf_op jit(solution)/shard_map/pallas_call | solution.py:63
  140.5 0.8 dynamic_slice.12
  141.2 2.4 divide_multiply_fusion
  143.6 0.6 fusion.23
  144.3 2.7 %copy.67 = f32[16,128,64]{0,1,2:T(8,128)} copy(f32[16,128,64]{1,2,0:T(8,128)S(1)} %fusion.23) | data formatting | bytes 1048576 | tf_op jit(solution)/shard_map/ts,nsk->ntk/dot_general | solution.py:298
  147.0 0.9 slice_bitcast_fusion
  148.2 0.6 fusion.25
  148.8 2.7 %copy.69 = f32[16,64,128]{0,2,1:T(8,128)} copy(f32[16,64,128]{2,1,0:T(8,128)S(1)} %bitcast.118) | data formatting | bytes 1048576 | tf_op jit(solution)/shard_map/reshape | solution.py:295
  151.6 2.6 copy.68
  154.2 7.1 %multiply_convert_fusion.1 = (bf16[16,64,128]{0,2,1:T(8,128)(2,1)S(1)}, bf16[16,64,128]{0,2,1:T(8,128)(2,1)}, bf16[16,64,128]{0,2,1:T(8,128)(2,1)}) fusion(f32[16,64,128]{0,2,1:T(8,128)} %copy.69, f32[16,128,64]{0,1,2:T(8,128)} %copy.67, f32[16,128]{0,1:T(8,128)S(1)} %slice_bitcast_fusion, f32[16,64,128]{0,2,1:T(8,128)} %copy.68), kind=kLoop, calls=%fused_computation.2 | loop fusion | flops 1048576 | bytes 2367488 | tf_op jit(solution)/shard_map/convert_element_type | solution.py:301
  161.2 2.7 %copy.70.q_ref = bf16[16,64,128]{2,1,0:T(8,128)(2,1)} copy(bf16[16,64,128]{0,2,1:T(8,128)(2,1)} %get-tuple-element.13) | data formatting | bytes 524288 | tf_op jit(solution)/shard_map/convert_element_type | solution.py:300
  164.0 1.5 subtract_exponential_fusion
  165.5 2.0 copy.73
  167.6 1.4 multiply_reduce_fusion.1
  169.0 0.6 pad_maximum_fusion.2.x_ref
  169.6 8.8 %shard_map.156 = f32[4,136,128]{2,1,0:T(8,128)} custom-call(f32[136,128]{1,0:T(8,128)} %pad_maximum_fusion.2.x_ref), custom_call_target="tpu_custom_call" | custom-call | tf_op jit(solution)/shard_map/pallas_call | solution.py:63
  178.4 1.3 exponential_bitcast_fusion.3
  179.8 1.0 copy.71
  180.7 1.7 fusion.19.state_ref
  182.4 2.6 shard_map.157
  185.0 1.5 multiply_reduce_fusion.2
  186.7 1.2 fusion.17
  187.9 0.6 constant_dynamic-slice_fusion.k_ref
  188.5 1.6 slice.84
  190.1 0.4 copy.81
  190.5 1.0 copy.78
  191.6 0.8 dynamic_slice.15
  192.3 0.8 dynamic_slice.14
  193.1 1.1 maximum_convert_fusion.x_ref
  194.2 5.8 %shard_map.158 = f32[1024,256]{1,0:T(8,128)} custom-call(f32[1056,256]{1,0:T(8,128)} %maximum_convert_fusion.x_ref, f32[31,256]{1,0:T(8,128)} %constant_dynamic-slice_fusion.k_ref), custom_call_target="tpu_custom_call" | custom-call | flops 16252928 | bytes 2097152 | tf_op jit(solution)/shard_map/pallas_call | solution.py:255
  199.9 1.6 fusion.30
  201.5 0.6 pad_maximum_fusion.3.x_ref
  202.1 6.5 %shard_map.159 = f32[8,2,1024]{2,1,0:T(2,128)} custom-call(f32[2,1024]{1,0:T(2,128)} %pad_maximum_fusion.3.x_ref), custom_call_target="tpu_custom_call" | custom-call | tf_op jit(solution)/shard_map/pallas_call | solution.py:63
  208.6 0.9 reduce_sum.83
  209.5 1.6 multiply_convert_fusion.3
  211.2 2.3 convolution_convert_fusion
  213.5 2.3 copy.89
  215.8 8.3 %shard_map.160 = bf16[2,4,128,2048]{3,2,1,0:T(8,128)(2,1)} custom-call(bf16[2,4,128,2048]{3,2,1,0:T(8,128)(2,1)} %bitcast.110), custom_call_target="tpu_custom_call" | custom-call | tf_op jit(solution)/shard_map/pallas_call | solution.py:63
  224.1 5.1 %reduce_sum.84.x_ref = bf16[4,128,2048]{2,1,0:T(8,128)(2,1)} reduce(bf16[2,4,128,2048]{3,2,1,0:T(8,128)(2,1)} %shard_map.160, bf16[]{:T(256)} %constant.77.clone.1), dimensions={0}, to_apply=%region_7.8 | reduce | flops 1048576 | bytes 6291458 | tf_op jit(solution)/shard_map/reduce_sum | solution.py:423
  229.2 29.0 %shard_map.161 = bf16[4,128,2048]{2,1,0:T(8,128)(2,1)} custom-call(bf16[4,128,2048]{2,1,0:T(8,128)(2,1)} %reduce_sum.84.x_ref), custom_call_target="tpu_custom_call" | custom-call | tf_op jit(solution)/shard_map/pallas_call | solution.py:63
  258.2 2.9 %reduce_sum.85 = bf16[128,2048]{1,0:T(8,128)(2,1)} reduce(bf16[4,128,2048]{2,1,0:T(8,128)(2,1)} %shard_map.161, bf16[]{:T(256)} %constant.77.clone.1), dimensions={0}, to_apply=%region_8.9 | reduce | flops 786432 | bytes 2621442 | tf_op jit(solution)/shard_map/reduce_sum | solution.py:425
  (47 shorter events, 1.1 us)
Async XLA Ops:
  0.0 187.9 %copy-start = (f32[31,1024]{1,0:T(8,128)S(1)}, f32[31,1024]{1,0:T(8,128)}, u32[]{:S(2)}) copy-start(f32[31,1024]{1,0:T(8,128)} %param.27) | copy-start | bytes 380932
  0.0 3.6 %copy-start.8 = (bf16[128,512]{1,0:T(8,128)(2,1)S(1)}, bf16[128,512]{1,0:T(8,128)(2,1)}, u32[]{:S(2)}) copy-start(bf16[128,512]{1,0:T(8,128)(2,1)} %param.20) | copy-start | bytes 393220
  0.0 3.9 %copy-start.9 = (bf16[128,512]{1,0:T(8,128)(2,1)S(1)}, bf16[128,512]{1,0:T(8,128)(2,1)}, u32[]{:S(2)}) copy-start(bf16[128,512]{1,0:T(8,128)(2,1)} %param.21) | copy-start | bytes 393220
  0.0 4.2 %copy-start.6 = (bf16[128,1024]{1,0:T(8,128)(2,1)S(1)}, bf16[128,1024]{1,0:T(8,128)(2,1)}, u32[]{:S(2)}) copy-start(bf16[128,1024]{1,0:T(8,128)(2,1)} %param.25) | copy-start | bytes 786436
  0.0 4.5 %copy-start.7 = (bf16[128,1024]{1,0:T(8,128)(2,1)S(1)}, bf16[128,1024]{1,0:T(8,128)(2,1)}, u32[]{:S(2)}) copy-start(bf16[128,1024]{1,0:T(8,128)(2,1)} %param.26) | copy-start | bytes 786436
  0.0 4.9 %copy-start.3 = (bf16[128,2048]{1,0:T(8,128)(2,1)S(1)}, bf16[128,2048]{1,0:T(8,128)(2,1)}, u32[]{:S(2)}) copy-start(bf16[128,2048]{1,0:T(8,128)(2,1)} %param.16) | copy-start | bytes 1572868
  4.7 0.7 copy-start.10
  124.2 19.5 %copy-start.2 = (bf16[1024,1024]{1,0:T(8,128)(2,1)}, bf16[1024,1024]{1,0:T(8,128)(2,1)S(1)}, u32[]{:S(2)}) copy-start(bf16[1024,1024]{1,0:T(8,128)(2,1)S(1)} %convolution_convert_fusion.1) | copy-start | bytes 6291460
  125.4 67.7 %collective-permute-start = (bf16[32,256]{1,0:T(8,128)(2,1)}, bf16[32,256]{1,0:T(8,128)(2,1)S(1)}, u32[]{:S(2)}, u32[]{:S(2)}) collective-permute-start(bf16[32,256]{1,0:T(8,128)(2,1)} %slice.93), channel_id=1, source_target_pairs={{0,8},{2,10},{4,12},{6,14},{8,16},{10,18},{12,20},{14,22},{16,24},... | collective-permute-start | bytes 49160 | tf_op jit(solution)/shard_map/ppermute | solution.py:394
  143.6 5.2 %copy-start.5 = (f32[1024,128]{1,0:T(8,128)S(1)}, f32[1024,128]{1,0:T(8,128)}, u32[]{:S(2)}) copy-start(f32[1024,128]{1,0:T(8,128)} %get-tuple-element.16) | copy-start | bytes 1572868
  147.0 4.6 %copy-start.4 = (f32[1024,128]{1,0:T(8,128)S(1)}, f32[1024,128]{1,0:T(8,128)}, u32[]{:S(2)}) copy-start(f32[1024,128]{1,0:T(8,128)} %get-tuple-element.18) | copy-start | bytes 1572868
  168.9 16.1 %copy-start.1 = (bf16[16,64,128]{2,1,0:T(8,128)(2,1)S(1)}, bf16[16,64,128]{2,1,0:T(8,128)(2,1)}, u32[]{:S(2)}) copy-start(bf16[16,64,128]{2,1,0:T(8,128)(2,1)} %copy.70.q_ref) | copy-start | bytes 786436
  180.7 5.9 %copy-start.11 = (f32[128]{0:T(128)S(1)}, f32[128]{0:T(128)}, u32[]{:S(2)}) copy-start(f32[128]{0:T(128)} %param.24) | copy-start | bytes 1540
